TPU v7x, 32 devices: a whole 2x2x4 slice. The times are simulated.
32 devices in a mesh: grp: 2 (over y), kv: 4 (over z), tp: 4 (over x, core).
Axes of the slice: x: 2, y: 2, z: 4, core: 2. Of those that a mesh axis runs over, the one named last changes fastest.
Arguments:
- tokens: bfloat16 [512, 8, 4096], P('kv', 'grp'), parts along dimension 1, may hold values from -72 to 72
- lengths: int32 [8], P('grp'), parts along dimension 0, may hold values from 1 to 512, 768 in all
- chosen: int32 [8, 32, 8, 8], P('grp', 'tp', 'kv'), parts along dimension 0, may hold values from -1 to 7, as said below
- w_query: bfloat16 [4096, 2048], P(None, 'tp'), may hold values from -0.09375 to 0.09375
- w_key: bfloat16 [4096, 2048], P(None, 'tp'), may hold values from -0.09375 to 0.09375
- w_value: bfloat16 [4096, 2048], P(None, 'tp'), may hold values from -0.09375 to 0.09375
- w_gate: bfloat16 [4096, 2, 32], P(None, None, 'tp'), may hold values from -0.09375 to 0.09375
- pool_weights: float32 [2, 32, 64], replicated, may hold values from -1 to 1
- w_out: bfloat16 [2048, 4096], P(None, 'tp'), may hold values from -0.5 to 0.5
Outputs:
- mixed: bfloat16 [512, 8, 4096], P(('kv', 'tp'), 'grp'), parts along dimension 1
There are 2 independent parts, one for each index of `grp`. A program takes and returns all parts, laid end to end along the dimension named above; an argument that names none is the same for every part. Nothing has to cross between parts.
Inputs may be any that keep to these rules, and one draw needn't show every extreme that they name: `chosen`: for query block b the live slots hold min(8, b+1) distinct blocks, all <= b, among them b, b-1 (when b >= 1) and 0; the other slots are -1.
All inputs are finite; a program needn't handle non-finite values.
Results may differ from a plain program's by a relative error of at most 0.014.
Values may be sent and summed in bfloat16 or wider, within the bound.
A program may use at most 128 MiB of HBM per device.

v0:
```python
from functools import partial

import jax
import jax.numpy as jnp
from jax import lax
from jax.sharding import PartitionSpec as P

HD = 64
QB = 64
L_CMP = 32


LOW_FILL = -1e30


def pooled_blocks(key_rows, pool_weight):
    row_count, seq_count, head_count, head_dim = key_rows.shape
    grouped = key_rows.reshape(row_count // L_CMP, L_CMP, seq_count, head_count, head_dim)
    return (grouped * pool_weight[None, :, None, None, :]).sum(1).astype(jnp.bfloat16)


def pooled_attend(queries, key_pooled, val_pooled, query_pos, lengths):
    head_dim = queries.shape[-1]
    cmp_end = jnp.arange(key_pooled.shape[0]) * L_CMP + L_CMP - 1
    scores = jnp.einsum(
        "qshd,cshd->shqc", queries, key_pooled, preferred_element_type=jnp.float32
    ) * head_dim ** (-0.5)
    usable = (cmp_end[None, None, :] <= query_pos[None, :, None]) & (
        cmp_end[None, None, :] < lengths[:, None, None]
    )
    usable = usable[:, None]
    row_top = jnp.max(jnp.where(usable, scores, LOW_FILL), axis=-1, keepdims=True)
    weights = jnp.where(usable, jnp.exp(scores - row_top), 0.0)
    totals = jnp.sum(weights, axis=-1)
    gathered = jnp.einsum(
        "shqc,cshd->shqd",
        weights.astype(jnp.bfloat16),
        val_pooled,
        preferred_element_type=jnp.float32,
    )
    return gathered / jnp.where(totals > 0, totals, 1.0)[..., None]


def fold_step(running, key_piece, begin_row, queries, chosen, query_pos, lengths):
    maxima, totals, weighted = running
    piece_keys, piece_values = key_piece
    head_dim = queries.shape[-1]
    key_pos = jnp.arange(piece_keys.shape[0])
    key_blk = key_pos // QB
    picked = jnp.any(chosen[..., None] == key_blk, axis=3)
    picked = jnp.repeat(picked, QB, axis=2)
    usable = (
        picked
        & (key_pos[None, None, None, :] <= query_pos[None, None, :, None])
        & (key_pos[None, None, None, :] < lengths[:, None, None, None])
    )
    scores = jnp.einsum(
        "qshd,kshd->shqk", queries, piece_keys, preferred_element_type=jnp.float32
    ) * head_dim ** (-0.5)
    new_max = jnp.maximum(maxima, jnp.max(jnp.where(usable, scores, LOW_FILL), axis=-1))
    weights = jnp.where(usable, jnp.exp(scores - new_max[..., None]), 0.0)
    shrink = jnp.exp(maxima - new_max)
    totals = jnp.sum(weights, axis=-1)
    weighted = jnp.einsum(
        "shqk,kshd->shqd",
        weights.astype(jnp.bfloat16),
        piece_values,
        preferred_element_type=jnp.float32,
    )
    return (new_max, totals, weighted)


def body(tokens, lengths, chosen, w_query, w_key, w_value, w_gate, pool_weights, w_out):
    row_count, seq_count, model_width = tokens.shape
    head_count = w_query.shape[1] // HD
    query_pos = lax.axis_index("kv") * row_count + jnp.arange(row_count)
    flat_rows = tokens.reshape(row_count * seq_count, model_width)

    def project(weight):
        product = jnp.dot(flat_rows, weight, preferred_element_type=jnp.float32)
        return product.astype(jnp.bfloat16).reshape(row_count, seq_count, head_count, HD)

    queries = project(w_query)
    key_rows = project(w_key)
    value_rows = project(w_value)
    gate_values = jax.nn.sigmoid(
        jnp.dot(
            flat_rows,
            w_gate.reshape(model_width, 2 * head_count),
            preferred_element_type=jnp.float32,
        )
    )
    gate_values = gate_values.reshape(row_count, seq_count, 2, head_count)
    key_pooled, val_pooled = (
        lax.all_gather(pooled_blocks(key_rows, pool_weights[0]), "kv", axis=0, tiled=True),
        lax.all_gather(pooled_blocks(value_rows, pool_weights[1]), "kv", axis=0, tiled=True),
    )
    start_state = (
        jnp.full((seq_count, head_count, row_count), LOW_FILL, jnp.float32),
        jnp.zeros((seq_count, head_count, row_count), jnp.float32),
        jnp.zeros((seq_count, head_count, row_count, HD), jnp.float32),
    )
    step_fn = partial(
        fold_step, queries=queries, chosen=chosen, query_pos=query_pos, lengths=lengths
    )
    maxima, totals, weighted = step_fn(
        start_state,
        (
            lax.all_gather(key_rows, "kv", axis=0, tiled=True),
            lax.all_gather(value_rows, "kv", axis=0, tiled=True),
        ),
        jnp.int32(0),
    )
    picked_out = weighted / jnp.where(totals > 0, totals, 1.0)[..., None]
    pooled_out = pooled_attend(queries, key_pooled, val_pooled, query_pos, lengths)
    combined = gate_values[:, :, 0, :, None] * pooled_out.transpose(2, 0, 1, 3) + gate_values[
        :, :, 1, :, None
    ] * picked_out.transpose(2, 0, 1, 3)
    live = query_pos[:, None] < lengths[None, :]
    attended = (
        jnp.where(live[:, :, None, None], combined, 0.0)
        .astype(jnp.bfloat16)
        .reshape(row_count, seq_count, head_count * HD)
    )
    group_count = lax.axis_size("tp")
    all_heads = lax.all_gather(attended, "tp", axis=2, tiled=True)
    group_width = head_count * HD
    col_width = w_out.shape[1]
    grouped_rows = all_heads.reshape(row_count * seq_count, group_count, group_width)
    grouped_weight = w_out.reshape(group_count, group_width, col_width)
    partial_cols = jnp.einsum(
        "rgk,gkc->rgc", grouped_rows, grouped_weight, preferred_element_type=jnp.float32
    )
    column_sum = jnp.sum(partial_cols.astype(jnp.bfloat16).astype(jnp.float32), axis=1)
    column_out = column_sum.astype(jnp.bfloat16).reshape(row_count, seq_count, col_width)
    return lax.all_to_all(column_out, "tp", split_axis=0, concat_axis=2, tiled=True)


def solution(mesh):
    placed = (
        P("kv", "grp", None),
        P("grp"),
        P("grp", "tp", "kv", None),
        P(None, "tp"),
        P(None, "tp"),
        P(None, "tp"),
        P(None, None, "tp"),
        P(),
        P(None, "tp"),
    )
    return jax.shard_map(
        body, mesh=mesh, in_specs=placed, out_specs=P(("kv", "tp"), "grp", None), check_vma=False
    )
```

profile of v0, /device:TPU:17, one launch (start us, length us, event | category | flops | bytes accessed | tf_op | source)
XLA Modules:
  0.0 179.1 jit_solution(17314178159223339070)
XLA Ops:
  6.5 7.0 %reshape.216 = bf16[512,4096]{1,0:T(8,128)(2,1)} reshape(bf16[128,4,4096]{2,1,0:T(4,128)(2,1)} %param.9) | data formatting | bytes 8388608 | tf_op jit(solution)/shard_map/reshape | solution.py:77
  13.5 5.8 %convolution_convert_fusion.1 = bf16[512,512]{1,0:T(8,128)(2,1)S(1)} fusion(bf16[512,4096]{1,0:T(8,128)(2,1)} %reshape.216, bf16[4096,512]{1,0:T(8,128)(2,1)} %param.13), kind=kOutput, calls=%fused_computation.19 | convolution fusion | flops 2147745792 | bytes 8912896 | tf_op jit(solution)/shard_map/dot_general | solution.py:80
  19.3 0.5 reshape.221
  19.8 1.9 %copy.57 = bf16[128,4,8,64]{0,3,2,1:T(8,128)(2,1)} copy(bf16[128,4,8,64]{3,2,1,0:T(8,128)(2,1)S(1)} %reshape.221) | data formatting | bytes 1048576 | tf_op jit(solution)/shard_map/reshape | solution.py:81
  21.8 5.8 %convolution_convert_fusion = bf16[512,512]{1,0:T(8,128)(2,1)S(1)} fusion(bf16[512,4096]{1,0:T(8,128)(2,1)} %reshape.216, bf16[4096,512]{1,0:T(8,128)(2,1)} %param.14), kind=kOutput, calls=%fused_computation.18 | convolution fusion | flops 2147745792 | bytes 8912896 | tf_op jit(solution)/shard_map/dot_general | solution.py:80
  27.6 0.5 reshape.222
  28.1 1.9 %copy.59 = bf16[128,4,8,64]{0,3,2,1:T(8,128)(2,1)} copy(bf16[128,4,8,64]{3,2,1,0:T(8,128)(2,1)S(1)} %reshape.222) | data formatting | bytes 1048576 | tf_op jit(solution)/shard_map/reshape | solution.py:81
  30.3 1.8 %reshape.228 = f32[4,32,4,8,64]{4,3,2,1,0:T(8,128)} reshape(bf16[512,512]{1,0:T(8,128)(2,1)S(1)} %convolution_convert_fusion) | data formatting | bytes 1572864 | tf_op jit(solution)/shard_map/convert_element_type | solution.py:19
  32.1 0.4 reshape.227
  32.6 3.5 %fusion.17 = f32[512,16]{0,1:T(8,128)S(1)} fusion(bf16[512,4096]{1,0:T(8,128)(2,1)} %reshape.216, bf16[4096,2,8]{0,2,1:T(8,128)(2,1)S(1)} %copy-done), kind=kOutput, calls=%fused_computation.30 | convolution fusion | flops 67133440 | bytes 4358144 | tf_op jit(solution)/shard_map/dot_general | solution.py:87
  36.2 0.3 reshape.218
  36.6 0.4 fusion.29
  37.2 5.9 %convolution_convert_fusion.2 = bf16[512,512]{1,0:T(8,128)(2,1)S(1)} fusion(bf16[512,4096]{1,0:T(8,128)(2,1)} %reshape.216, bf16[4096,512]{1,0:T(8,128)(2,1)} %param.12), kind=kOutput, calls=%fused_computation.20 | convolution fusion | flops 2147745792 | bytes 8912896 | tf_op jit(solution)/shard_map/dot_general | solution.py:80
  43.1 1.5 reshape.219
  44.6 2.2 %copy.53 = bf16[128,4,8,64]{0,3,2,1:T(8,128)(2,1)S(1)} copy(bf16[128,4,8,64]{3,2,1,0:T(8,128)(2,1)} %reshape.219) | data formatting | bytes 1048576 | tf_op jit(solution)/shard_map/reshape | solution.py:81
  46.8 1.9 %multiply_reduce_fusion = bf16[4,4,8,64]{3,2,1,0:T(8,128)(2,1)S(1)} fusion(f32[4,32,4,8,64]{4,3,2,1,0:T(8,128)} %reshape.228, f32[32,64]{1,0:T(8,128)S(1)} %get-tuple-element.9), kind=kLoop, calls=%fused_computation.9 | loop fusion | flops 516096 | bytes 1073152 | tf_op jit(solution)/shard_map/reduce_sum | solution.py:19
  48.7 14.4 %all_gather.16 = bf16[16,4,8,64]{3,2,1,0:T(8,128)(2,1)S(1)} all-gather(bf16[4,4,8,64]{3,2,1,0:T(8,128)(2,1)S(1)} %multiply_reduce_fusion), channel_id=1, replica_groups=mesh['grp'=2,'kv'=4,'tp'=4] {'kv'}, dimensions={0}, use_global_device_ids=true | all-gather | bytes 81920 | tf_op jit(solution)/shard_map/all_gather | solution.py:96
  63.4 14.7 %all_gather.15 = bf16[16,4,8,64]{3,2,1,0:T(8,128)(2,1)S(1)} all-gather(bf16[4,4,8,64]{3,2,1,0:T(8,128)(2,1)S(1)} %multiply_reduce_fusion.1), channel_id=1, replica_groups=mesh['grp'=2,'kv'=4,'tp'=4] {'kv'}, dimensions={0}, use_global_device_ids=true | all-gather | bytes 81920 | tf_op jit(solution)/shard_map/all_gather | solution.py:95
  78.0 0.5 compare_reduce_fusion
  79.4 4.3 %select_reduce_fusion = (f32[4,8,128]{2,1,0:T(8,128)S(1)}, f32[4,8,128,512]{3,2,1,0:T(8,128)S(1)}) fusion(pred[4,512]{1,0:T(4,128)(4,1)S(1)} %iota_compare_fusion.1, pred[128,512]{1,0:T(8,128)(4,1)S(1)} %iota_compare_fusion, pred[4,8,2,512]{3,2,1,0:T(4,128)(4,1)S(1)} %compare_reduce_fusion, bf16[128,4,8,64]{0,3,2,1:T(8,128)(2,1)S(1)} %copy.53, ...), kind=kOutput, calls=%fused_computation.2 | convolution fusion | flops 278917120 | bytes 11126784 | tf_op jit(solution)/shard_map/qshd,kshd->shqk/dot_general | solution.py:57
  83.8 4.5 %fusion.2 = (f32[4,8,128]{2,1,0:T(8,128)S(1)}, bf16[4,8,128,512]{3,2,1,0:T(8,128)(2,1)}) fusion(f32[4,8,128,512]{3,2,1,0:T(8,128)S(1)} %get-tuple-element.12, f32[4,8,128]{2,1,0:T(8,128)S(1)} %broadcast_maximum_fusion, pred[4,512]{1,0:T(4,128)(4,1)S(1)} %iota_compare_fusion.1, pred[128,512]{1,0:T(8,128)(4,1)S(1)} %iota_compare_fusion, ...), kind=kLoop, calls=%fused_computation.5 | loop fusion | flops 14675968 | bytes 12716032 | tf_op jit(solution)/shard_map/reduce_sum | solution.py:63
  88.3 25.5 %all-gather.6.cloned.1.call-done = bf16[512,4,8,64]{0,3,2,1:T(8,128)(2,1)} async-done(((bf16[128,4,8,64]{0,3,2,1:T(8,128)(2,1)}), bf16[512,4,8,64]{0,3,2,1:T(8,128)(2,1)}) %all-gather.6.cloned.1.call-update) | async-done | bytes 2097168 | tf_op jit(solution)/shard_map/all_gather | solution.py:110
  113.8 4.4 %fusion.11 = f32[128,4,8,64]{0,3,2,1:T(8,128)S(1)} fusion(bf16[4,8,128,512]{3,2,1,0:T(8,128)(2,1)} %get-tuple-element.6, bf16[512,4,8,64]{0,3,2,1:T(8,128)(2,1)} %all-gather.6.cloned.1.call-done, f32[128,4,8]{0,2,1:T(8,128)S(1)} %compare_select_fusion, f32[128,4,8]{0,2,1:T(8,128)S(1)} %copy.56), kind=kOutput, calls=%fused_computation.22 | convolution fusion | flops 268959744 | bytes 7372800 | tf_op jit(solution)/shard_map/shqk,kshd->shqd/dot_general | solution.py:64
  118.2 0.4 fusion.9
  118.6 1.2 copy.60
  119.8 25.6 %all-gather.8.cloned.1.call-done = bf16[128,4,2048]{2,1,0:T(4,128)(2,1)} async-done(((bf16[128,4,512]{2,1,0:T(4,128)(2,1)}), bf16[128,4,2048]{2,1,0:T(4,128)(2,1)}) %all-gather.8.cloned.1.call-update) | async-done | bytes 2097168 | tf_op jit(solution)/shard_map/all_gather | solution.py:126
  145.5 3.1 %reshape.224 = bf16[512,4,512]{2,1,0:T(4,128)(2,1)S(1)} reshape(bf16[128,4,2048]{2,1,0:T(4,128)(2,1)} %all-gather.8.cloned.1.call-done) | data formatting | bytes 4194304 | tf_op jit(solution)/shard_map/reshape | solution.py:129
  148.6 4.6 %convert_reduce_fusion = bf16[512,1024]{1,0:T(8,128)(2,1)S(1)} fusion(bf16[4,512,1024]{2,1,0:T(8,128)(2,1)} %bitcast.66, bf16[512,4,512]{2,1,0:T(4,128)(2,1)S(1)} %reshape.224), kind=kOutput, calls=%fused_computation.7 | convolution fusion | flops 2151153664 | bytes 7340032 | tf_op jit(solution)/shard_map/rgk,gkc->rgc/dot_general | solution.py:131
  153.3 0.4 reshape.226
  153.7 16.1 %all_to_all.18 = bf16[128,4,1024]{2,1,0:T(4,128)(2,1)S(1)} all-to-all(bf16[128,4,1024]{2,1,0:T(4,128)(2,1)S(1)} %reshape.226), channel_id=1, replica_groups=mesh['grp'=2,'kv'=4,'tp'=4] {'tp'}, dimensions={0} | all-to-all | bytes 2097152 | tf_op jit(solution)/shard_map/all_to_all | solution.py:136
  170.1 0.8 copy.65
  170.9 1.6 reshape.229
  (37 shorter events, 2.2 us)
Async XLA Ops:
  6.5 26.1 %copy-start = (bf16[4096,2,8]{0,2,1:T(8,128)(2,1)S(1)}, bf16[4096,2,8]{0,2,1:T(8,128)(2,1)}, u32[]{:S(2)}) copy-start(bf16[4096,2,8]{0,2,1:T(8,128)(2,1)} %param.15) | copy-start | bytes 393220
  6.5 72.9 %all-gather.4.cloned.1.call-start = ((), (), s32[]{:S(2)}) async-start(), calls=%async_computation.1 | async-start | bytes 2621440 | tf_op jit(solution)/shard_map/all_gather | solution.py:109
  21.7 92.1 %all-gather.6.cloned.1.call-start = ((), (), s32[]{:S(2)}) async-start(), calls=%async_computation.2 | async-start | bytes 2621440 | tf_op jit(solution)/shard_map/all_gather | solution.py:110
  27.6 5.0 %copy-start.3 = (f32[2,32,64]{2,1,0:T(8,128)S(1)}, f32[2,32,64]{2,1,0:T(8,128)}, u32[]{:S(2)}) copy-start(f32[2,32,64]{2,1,0:T(8,128)} %param.16) | copy-start | bytes 49156
  30.1 115.4 %all-gather.8.cloned.1.call-start = ((), (), s32[]{:S(2)}) async-start(), calls=%async_computation.3 | async-start | bytes 2621440 | tf_op jit(solution)/shard_map/all_gather | solution.py:126
  43.0 35.0 %copy-start.2 = (s32[4,8,2,8]{3,2,1,0:T(2,128)S(1)}, s32[4,8,2,8]{3,2,1,0:T(2,128)}, u32[]{:S(2)}) copy-start(s32[4,8,2,8]{3,2,1,0:T(2,128)} %param.11) | copy-start | bytes 6148
  43.0 35.5 %copy-start.4 = (s32[4]{0:T(128)S(1)}, s32[4]{0:T(128)}, u32[]{:S(2)}) copy-start(s32[4]{0:T(128)} %param.10) | copy-start | bytes 52
  153.3 19.3 %copy-start.1 = (bf16[4096,2,8]{0,2,1:T(8,128)(2,1)S(1)}, bf16[4096,2,8]{0,2,1:T(8,128)(2,1)}, u32[]{:S(2)}) copy-start(bf16[4096,2,8]{0,2,1:T(8,128)(2,1)} %param.15) | copy-start | bytes 393220
Sparse Core Ops, SparseCore 0:
  21.9 46.4 all-gather.3
  69.9 43.8 all-gather.5
  120.0 25.4 all-gather.7
where the time goes:
time: 182 us; the launch traced here: 179 us
  waiting for transfers between devices  51.2 us (28%)
  blocking collectives  45.1 us (25%)
  matrix products  34.9 us (19%)
  local copies, waits for them, and re-layouts  26.4 us (15%)
  between operations  13.4 us (7%)
  other arithmetic  7.74 us (4%)
    all_gather x1, waiting for transfers between devices, body(): all_heads = lax.all_gather(attended, 'tp', axis=2, tiled=True)  25.6 us
    all_gather x1, waiting for transfers between devices, body(): lax.all_gather(value_rows, 'kv', axis=0, tiled=True)  25.5 us
    dot_general x3, matrix products, project(): product = jnp.dot(flat_rows, weight, preferred_element_type=jnp.float32)  17.4 us
    all_to_all x1, blocking collectives, body(): lax.all_to_all(column_out, 'tp', split_axis=0, concat_axis=2, tiled=True)  16.1 us
    all_gather x1, blocking collectives, body(): lax.all_gather(pooled_blocks(key_rows, pool_weights[0]), 'kv', axis=0, ti...  14.7 us
    all_gather x1, blocking collectives, body(): lax.all_gather(pooled_blocks(value_rows, pool_weights[1]), 'kv', axis=0,...  14.4 us
    reshape x6, local copies, waits for them, and re-layouts, project(): product.astype(jnp.bfloat16).reshape(row_count, seq_count, head_count, HD)  8.64 us
    reshape x1, local copies, waits for them, and re-layouts, body(): flat_rows = tokens.reshape(row_count * seq_count, model_width)  6.95 us
  transfers between devices with their start and end apart: 3, of which 2 were waited for; matrix products, arithmetic and copies ran while one was open for 21% of the time, Pallas kernels for 0%

commit v1 on v0

v1 whole, which is shorter than its diff:
```python
import functools

import jax
import jax.numpy as jnp
from jax import lax
from jax.experimental import pallas as pl
from jax.experimental.pallas import tpu as pltpu
from jax.sharding import PartitionSpec as P

HD = 64
QB = 64
L_CMP = 32
PAD = 16
LOW = -1e30
FLOOR = -1e29
MESH = pl.DeviceIdType.MESH
NT = (((1,), (1,)), ((), ()))


def rank_slots(seq_count, seq_len, rows, shards):
    total = seq_count * seq_len * 3 // 8
    slots = []
    for r in range(seq_count):
        most = min(seq_len, (total - (seq_count - 1 - r)) // (r + 1))
        slots.append(min(shards, -(-most // rows)))
    return slots


def project_kernel(
    rank_ref, len_ref, base_ref, x_ref, wq_ref, wk_ref, wv_ref, wg_ref, pool_ref,
    q_ref, kv_ref, g_ref, acc, gacc,
):
    step = pl.program_id(0)
    width = wq_ref.shape[1]
    x = x_ref[...]

    @pl.when(step == 0)
    def _():
        acc[...] = jnp.zeros_like(acc)
        gacc[...] = jnp.zeros_like(gacc)

    for n, w in enumerate((wq_ref, wk_ref, wv_ref)):
        acc[:, n * width : (n + 1) * width] += jnp.dot(
            x, w[...], preferred_element_type=jnp.float32
        )
    gacc[...] += jnp.dot(x, wg_ref[...], preferred_element_type=jnp.float32)

    @pl.when(step == pl.num_programs(0) - 1)
    def _():
        seqs, rows, _ = q_ref.shape
        pool = pool_ref[...]
        for s in range(seqs):
            at = rank_ref[s]
            span = slice(s * rows, (s + 1) * rows)
            q = acc[span, :width].astype(jnp.bfloat16)
            q_ref[at] = q * jnp.bfloat16(HD**-0.5)
            kv = acc[span, width:].astype(jnp.bfloat16)
            kv_ref[at, :rows, :] = kv
            grouped = kv.astype(jnp.float32).reshape(rows // L_CMP, L_CMP, 2 * width)
            pooled = (grouped * pool[None]).sum(1)
            fill = jnp.zeros((PAD - rows // L_CMP, 2 * width), jnp.float32)
            kv_ref[at, rows:, :] = jnp.concatenate([pooled, fill], 0).astype(jnp.bfloat16)
            gate = jax.nn.sigmoid(gacc[span, :])
            pos = base_ref[0] + lax.broadcasted_iota(jnp.int32, gate.shape, 0)
            g_ref[at] = jnp.where(pos < len_ref[s], gate, 0.0)


def mixer_kernel(
    slots, shards, ntp,
    q_ref, kv_ref, g_ref, bias_ref, pbias_ref, w_hbm,
    out_ref,
    items, att, mixed, pools, acc, top, tot, w_vmem,
    w_sem, z_send, z_recv, a_send, a_recv, o_send, o_recv,
):
    seqs, rows, width = q_ref.shape
    heads = width // HD
    pairs = heads // 2
    blocks = rows // QB
    chips = ntp // 2
    col = w_hbm.shape[1]
    part = rows // ntp
    i = lax.axis_index("kv")
    t = lax.axis_index("tp")
    x, c = t // 2, t % 2
    mate = x * 2 + (1 - c)

    w_copy = pltpu.make_async_copy(w_hbm, w_vmem, w_sem)
    w_copy.start()
    pools[...] = jnp.zeros_like(pools)

    def active(shard):
        count = 0
        for n in slots:
            count = count + jnp.where(shard < n, 1, 0)
        return count

    mine = active(i)
    after = active(i + 1)

    barrier = pltpu.get_barrier_semaphore()
    for d in range(1, ntp):
        pl.semaphore_signal(
            barrier, inc=1, device_id={"tp": lax.rem(t + d, ntp)}, device_id_type=MESH
        )

    @pl.when(i > 0)
    def _():
        pl.semaphore_signal(barrier, inc=1, device_id={"kv": i - 1}, device_id_type=MESH)

    @pl.when(i < shards - 1)
    def _():
        pl.semaphore_signal(barrier, inc=1, device_id={"kv": i + 1}, device_id_type=MESH)

    expected = ntp - 1 + jnp.where(i > 0, 1, 0) + jnp.where(i < shards - 1, 1, 0)
    pl.semaphore_wait(barrier, expected)

    def own_copy(r):
        return pltpu.make_async_remote_copy(
            src_ref=kv_ref.at[r], dst_ref=items.at[r, i],
            send_sem=z_send.at[r, i], recv_sem=z_recv.at[r, i],
            device_id={"kv": i + 1}, device_id_type=MESH,
        )

    def relay_copy(r, j):
        return pltpu.make_async_remote_copy(
            src_ref=items.at[r, j], dst_ref=items.at[r, j],
            send_sem=z_send.at[r, j], recv_sem=z_recv.at[r, j],
            device_id={"kv": i + 1}, device_id_type=MESH,
        )

    def block_copy(r, k, block, target):
        return pltpu.make_async_remote_copy(
            src_ref=att.at[r, block], dst_ref=att.at[r, block],
            send_sem=a_send.at[r, k], recv_sem=a_recv.at[r, k],
            device_id={"tp": target}, device_id_type=MESH,
        )

    def side(d):
        return lax.rem(x + d, chips) * 2 + c

    def origin(d):
        return lax.rem(x + chips - d, chips) * 2

    def out_copy(r, d):
        target = lax.rem(t + d, ntp)
        return pltpu.make_async_remote_copy(
            src_ref=mixed.at[r, pl.ds(pl.multiple_of(target * part, part), part), :],
            dst_ref=out_ref.at[r, :, pl.ds(pl.multiple_of(t * col, col), col)],
            send_sem=o_send.at[r, d], recv_sem=o_recv.at[r, d],
            device_id={"tp": target}, device_id_type=MESH,
        )

    def send_own(r, carry):
        own_copy(r).start()
        return carry

    lax.fori_loop(0, after, send_own, 0)

    lane = lax.broadcasted_iota(jnp.int32, (rows, 2 * HD), 1)
    first = lane < HD

    def pair_queries(r, p):
        q = q_ref[r, :, p * 2 * HD : (p + 1) * 2 * HD]
        zero = jnp.zeros_like(q)
        return jnp.concatenate([jnp.where(first, q, zero), jnp.where(first, zero, q)], 0)

    def scores_of(r, p, keys, bias):
        scores = lax.dot_general(
            pair_queries(r, p), keys, NT, preferred_element_type=jnp.float32
        )
        return scores + bias

    def block_bias(r, j, p):
        lines = [
            jnp.broadcast_to(bias_ref[r, j, n : n + 1, :], (QB, rows))
            for n in range(p * 2 * blocks, (p + 1) * 2 * blocks)
        ]
        return jnp.concatenate(lines, 0)

    def columns(p):
        return slice(p * 2 * HD, (p + 1) * 2 * HD)

    def value_columns(p):
        return slice(width + p * 2 * HD, width + (p + 1) * 2 * HD)

    def attend(r):
        row = lax.broadcasted_iota(jnp.int32, (2 * rows, rows), 0)
        row = jnp.where(row >= rows, row - rows, row)
        key = lax.broadcasted_iota(jnp.int32, (2 * rows, rows), 1)
        causal = jnp.where(key <= row, 0.0, LOW)
        pools[pl.ds(pl.multiple_of(i * PAD, PAD), PAD), :] = kv_ref[r, rows:, :]
        for p in range(pairs):
            bias = block_bias(r, i, p) + causal
            scores = scores_of(r, p, kv_ref[r, :rows, columns(p)], bias)
            peak = jnp.maximum(jnp.max(scores, axis=1, keepdims=True), FLOOR)
            e = jnp.exp(scores - peak)
            top[p] = jnp.broadcast_to(peak, (2 * rows, 2 * HD))
            tot[p] = jnp.broadcast_to(jnp.sum(e, axis=1, keepdims=True), (2 * rows, 2 * HD))
            acc[p] = jnp.dot(
                e.astype(jnp.bfloat16), kv_ref[r, :rows, value_columns(p)],
                preferred_element_type=jnp.float32,
            )

        def chunk(j, carry):
            pools[pl.ds(pl.multiple_of(j * PAD, PAD), PAD), :] = items[r, j, rows:, :]
            for p in range(pairs):
                scores = scores_of(
                    r, p, items[r, j, :rows, columns(p)], block_bias(r, j, p)
                )
                old = top[p]
                peak = jnp.maximum(old, jnp.max(scores, axis=1, keepdims=True))
                shrink = jnp.exp(old - peak)
                e = jnp.exp(scores - peak[:, :1])
                top[p] = peak
                tot[p] = tot[p] * shrink + jnp.sum(e, axis=1, keepdims=True)
                acc[p] = acc[p] * shrink + jnp.dot(
                    e.astype(jnp.bfloat16), items[r, j, :rows, value_columns(p)],
                    preferred_element_type=jnp.float32,
                )
            return carry

        lax.fori_loop(0, i, chunk, 0)

        pbias = pbias_ref[r]
        pbias = jnp.concatenate([pbias, pbias], 0)
        for p in range(pairs):
            scores = scores_of(r, p, pools[:, columns(p)], pbias)
            peak = jnp.maximum(jnp.max(scores, axis=1, keepdims=True), FLOOR)
            e = jnp.exp(scores - peak)
            total = jnp.sum(e, axis=1, keepdims=True)
            pooled = jnp.dot(
                e.astype(jnp.bfloat16), pools[:, value_columns(p)],
                preferred_element_type=jnp.float32,
            ) / jnp.where(total > 0, total, 1.0)
            picked_total = tot[p]
            picked = acc[p] / jnp.where(picked_total > 0, picked_total, 1.0)
            halves = []
            for side_at in range(2):
                h = 2 * p + side_at
                span = slice(side_at * rows, (side_at + 1) * rows)
                halves.append(
                    g_ref[r, :, h : h + 1] * pooled[span]
                    + g_ref[r, :, heads + h : heads + h + 1] * picked[span]
                )
            att[r, t, :, columns(p)] = jnp.where(first, halves[0], halves[1]).astype(
                jnp.bfloat16
            )

    def step(r, carry):
        @pl.when(r < mine)
        def _():
            def arrive(n, inner):
                j = i - 1 - n
                relay_copy(r, j).wait_recv()

                @pl.when(r < after)
                def _():
                    relay_copy(r, j).start()

                return inner

            lax.fori_loop(0, i, arrive, 0)
            attend(r)
            for d in range(1, chips):
                block_copy(r, d, t, side(d)).start()
            block_copy(r, 0, t, mate).start()

        @pl.when(r >= 1)
        def _():
            b = r - 1
            for d in range(1, chips):
                block_copy(b, d, origin(d) + c, mate).wait_recv()
                block_copy(b, chips - 1 + d, origin(d) + c, mate).start()
            block_copy(b, 0, mate, mate).wait_recv()
            for d in range(1, chips):
                block_copy(b, chips - 1 + d, origin(d) + 1 - c, mate).wait_recv()

            @pl.when(r == 1)
            def _():
                w_copy.wait()

            total = jnp.dot(att[b, 0], w_vmem[:width, :], preferred_element_type=jnp.float32)
            for g in range(1, ntp):
                total = total + jnp.dot(
                    att[b, g], w_vmem[g * width : (g + 1) * width, :],
                    preferred_element_type=jnp.float32,
                )
            mixed[b] = total.astype(jnp.bfloat16)
            for d in range(1, ntp):
                out_copy(b, d).start()
            out_ref[b, :, pl.ds(pl.multiple_of(t * col, col), col)] = mixed[
                b, pl.ds(pl.multiple_of(t * part, part), part), :
            ]

        return carry

    lax.fori_loop(0, mine + 1, step, 0)

    def blank(r, carry):
        out_ref[r] = jnp.zeros(out_ref.shape[1:], out_ref.dtype)
        return carry

    lax.fori_loop(mine, seqs, blank, 0)

    def finish(r, carry):
        for d in range(1, ntp):
            out_copy(r, d).wait_send()
            source = lax.rem(t + ntp - d, ntp)
            pltpu.make_async_remote_copy(
                src_ref=mixed.at[r, :part, :],
                dst_ref=out_ref.at[r, :, pl.ds(pl.multiple_of(source * col, col), col)],
                send_sem=o_send.at[r, d], recv_sem=o_recv.at[r, d],
                device_id={"tp": source}, device_id_type=MESH,
            ).wait_recv()
        block_copy(r, 0, t, mate).wait_send()
        for d in range(1, chips):
            block_copy(r, d, t, side(d)).wait_send()
            block_copy(r, chips - 1 + d, origin(d) + c, mate).wait_send()
        return carry

    lax.fori_loop(0, mine, finish, 0)

    def sent(r, carry):
        own_copy(r).wait_send()

        def relayed(j, inner):
            relay_copy(r, j).wait_send()
            return inner

        lax.fori_loop(0, i, relayed, 0)
        return carry

    lax.fori_loop(0, after, sent, 0)


def body(tokens, lengths, chosen, w_query, w_key, w_value, w_gate, pool_weights, w_out):
    rows, seqs, model = tokens.shape
    width = w_query.shape[1]
    heads = width // HD
    col = w_out.shape[1]
    shards = lax.axis_size("kv")
    ntp = lax.axis_size("tp")
    shard = lax.axis_index("kv")
    base = (shard * rows).astype(jnp.int32)
    blocks = rows // QB
    slots = rank_slots(seqs, rows * shards, rows, shards)

    ids = jnp.arange(seqs)
    ahead = (lengths[None, :] > lengths[:, None]) | (
        (lengths[None, :] == lengths[:, None]) & (ids[None, :] < ids[:, None])
    )
    rank = jnp.sum(ahead.astype(jnp.int32), axis=1)
    order = rank[None, :] == ids[:, None]
    sorted_len = jnp.sum(jnp.where(order, lengths[None, :], 0), axis=1)
    ranked = jnp.sum(jnp.where(order[:, :, None, None, None], chosen[None], 0), axis=1)

    block_ids = jnp.arange(shards * blocks)
    picked = jnp.any(ranked[..., None] == block_ids, axis=3)
    picked = picked.reshape(seqs, heads * blocks, shards, blocks).transpose(0, 2, 1, 3)
    picked = jnp.repeat(picked, QB, axis=3)
    key_pos = (jnp.arange(shards) * rows)[:, None] + jnp.arange(rows)[None, :]
    near = key_pos[None, :, None, :] < sorted_len[:, None, None, None]
    bias = jnp.where(picked & near, 0.0, LOW).astype(jnp.float32)

    slot = jnp.arange(shards * PAD)
    inner = slot % PAD
    end = (slot // PAD) * rows + inner * L_CMP + L_CMP - 1
    pos = base + jnp.arange(rows)
    usable = (
        (inner < rows // L_CMP)[None, None, :]
        & (end[None, None, :] <= pos[None, :, None])
        & (end[None, None, :] < sorted_len[:, None, None])
    )
    pbias = jnp.where(usable, 0.0, LOW).astype(jnp.float32)
    pool = jnp.concatenate(
        [jnp.tile(pool_weights[0], (1, heads)), jnp.tile(pool_weights[1], (1, heads))], 1
    )

    flat = tokens.transpose(1, 0, 2).reshape(seqs * rows, model)
    gate_w = w_gate.reshape(model, 2 * heads)
    depth = model // 8
    whole = lambda k, *_: (0, 0)
    q, kv, gates = pl.pallas_call(
        project_kernel,
        grid_spec=pltpu.PrefetchScalarGridSpec(
            num_scalar_prefetch=3,
            grid=(model // depth,),
            in_specs=[
                pl.BlockSpec((seqs * rows, depth), lambda k, *_: (0, k)),
                pl.BlockSpec((depth, width), lambda k, *_: (k, 0)),
                pl.BlockSpec((depth, width), lambda k, *_: (k, 0)),
                pl.BlockSpec((depth, width), lambda k, *_: (k, 0)),
                pl.BlockSpec((depth, 2 * heads), lambda k, *_: (k, 0)),
                pl.BlockSpec((L_CMP, 2 * width), whole),
            ],
            out_specs=[
                pl.BlockSpec((seqs, rows, width), lambda k, *_: (0, 0, 0)),
                pl.BlockSpec((seqs, rows + PAD, 2 * width), lambda k, *_: (0, 0, 0)),
                pl.BlockSpec((seqs, rows, 2 * heads), lambda k, *_: (0, 0, 0)),
            ],
            scratch_shapes=[
                pltpu.VMEM((seqs * rows, 3 * width), jnp.float32),
                pltpu.VMEM((seqs * rows, 2 * heads), jnp.float32),
            ],
        ),
        out_shape=[
            jax.ShapeDtypeStruct((seqs, rows, width), jnp.bfloat16),
            jax.ShapeDtypeStruct((seqs, rows + PAD, 2 * width), jnp.bfloat16),
            jax.ShapeDtypeStruct((seqs, rows, 2 * heads), jnp.float32),
        ],
        compiler_params=pltpu.CompilerParams(vmem_limit_bytes=48 * 2**20),
    )(rank, lengths, base[None], flat, w_query, w_key, w_value, gate_w, pool)

    chips = ntp // 2
    vmem = pl.BlockSpec(memory_space=pltpu.VMEM)
    dma = pltpu.SemaphoreType.DMA
    out = pl.pallas_call(
        functools.partial(mixer_kernel, slots, shards, ntp),
        out_shape=jax.ShapeDtypeStruct((seqs, rows // ntp, ntp * col), jnp.bfloat16),
        in_specs=[vmem] * 5 + [pl.BlockSpec(memory_space=pl.ANY)],
        out_specs=vmem,
        scratch_shapes=[
            pltpu.VMEM((seqs, shards, rows + PAD, 2 * width), jnp.bfloat16),
            pltpu.VMEM((seqs, ntp, rows, width), jnp.bfloat16),
            pltpu.VMEM((seqs, rows, col), jnp.bfloat16),
            pltpu.VMEM((shards * PAD, 2 * width), jnp.bfloat16),
            pltpu.VMEM((heads // 2, 2 * rows, 2 * HD), jnp.float32),
            pltpu.VMEM((heads // 2, 2 * rows, 2 * HD), jnp.float32),
            pltpu.VMEM((heads // 2, 2 * rows, 2 * HD), jnp.float32),
            pltpu.VMEM(w_out.shape, jnp.bfloat16),
            dma,
            dma((seqs, shards)),
            dma((seqs, shards)),
            dma((seqs, 2 * chips)),
            dma((seqs, 2 * chips)),
            dma((seqs, ntp)),
            dma((seqs, ntp)),
        ],
        compiler_params=pltpu.CompilerParams(
            collective_id=0, has_side_effects=True, vmem_limit_bytes=56 * 2**20
        ),
    )(q, kv, gates, bias, pbias, w_out)
    parts = [lax.dynamic_index_in_dim(out, rank[s], 0, keepdims=False) for s in range(seqs)]
    return jnp.stack(parts, axis=1)


def solution(mesh):
    placed = (
        P("kv", "grp", None),
        P("grp"),
        P("grp", "tp", "kv", None),
        P(None, "tp"),
        P(None, "tp"),
        P(None, "tp"),
        P(None, None, "tp"),
        P(),
        P(None, "tp"),
    )
    return jax.shard_map(
        body, mesh=mesh, in_specs=placed, out_specs=P(("kv", "tp"), "grp", None), check_vma=False
    )
```

time: 182 us -> 87.6 us (0.48)
  the two profiles are of different devices: /device:TPU:17 before, /device:TPU:25 now
where the time goes in v1:
time: 87.6 us; the launch traced here: 87.1 us
  Pallas kernels  61.4 us (70%)
  local copies, waits for them, and re-layouts  14.7 us (17%)
  between operations  7.77 us (9%)
  other arithmetic  3.2 us (4%)
    pallas_call x1, Pallas kernels, body(): pl.pallas_call(functools.partial(mixer_kernel, slots, shards, ntp), out_s...  47.9 us
    pallas_call x1, Pallas kernels, body(): pl.pallas_call(project_kernel, grid_spec=pltpu.PrefetchScalarGridSpec(num...  13.4 us
    transpose x1, local copies, waits for them, and re-layouts, body(): flat = tokens.transpose(1, 0, 2).reshape(seqs * rows, model)  6.45 us
    another operation x2, local copies, waits for them, and re-layouts, body(): return jnp.stack(parts, axis=1)  3.05 us
    unnamed x13, local copies, waits for them, and re-layouts  2.51 us

profile of v1, /device:TPU:25, one launch (start us, length us, event | category | flops | bytes accessed | tf_op | source)
XLA Modules:
  0.0 87.1 jit_solution(4513880909860033061)
XLA Ops:
  0.0 0.9 %convert_reduce_fusion.rank_ref = s32[4]{0:T(128)S(1)} fusion(s32[4]{0:T(128)} %len_ref.1), kind=kLoop, calls=%fused_computation.18 | loop fusion | flops 108 | bytes 32 | tf_op jit(solution)/shard_map/reduce_sum | solution.py:352
  0.9 0.7 slice_bitcast_fusion.1
  1.7 0.1 tile.22
  1.8 0.1 tile.25
  1.9 0.0 copy-start.4
  1.9 0.0 copy-start.3
  1.9 6.4 %copy.16 = bf16[4,128,4096]{2,1,0:T(8,128)(2,1)} copy(bf16[4,128,4096]{2,0,1:T(4,128)(2,1)} %bitcast.23) | data formatting | bytes 8388608 | tf_op jit(solution)/shard_map/transpose | solution.py:379
  8.4 0.0 copy-done.4
  8.4 0.5 copy.17.wg_ref
  8.9 0.0 copy-start.5
  8.9 13.4 %shard_map.91 = (bf16[4,128,512]{2,1,0:T(8,128)(2,1)S(1)}, bf16[4,144,1024]{2,1,0:T(8,128)(2,1)S(1)}, f32[4,128,16]{2,1,0:T(8,128)S(1)}) custom-call(s32[4]{0:T(128)S(1)} %convert_reduce_fusion.rank_ref, s32[4]{0:T(128)S(1)} %copy-done.3, s32[1]{0:T(128)} %bitcast.base_ref, bf16[512,4096]{1,0:T(8,128)(2,1)} %bitcast.22, bf16[4096,512]{1,0:T(8,128)(2,1)} %wq_ref.1, ...), custom_call_target="tpu_custom_call" | custom-call | tf_op jit(solution)/shard_map/pallas_call | solution.py:383
  22.3 0.0 copy-start
  22.4 1.0 %copy-done = bf16[4,144,1024]{2,1,0:T(8,128)(2,1)} copy-done((bf16[4,144,1024]{2,1,0:T(8,128)(2,1)}, bf16[4,144,1024]{2,1,0:T(8,128)(2,1)S(1)}, u32[]{:S(2)}) %copy-start) | copy-done | bytes 1179672
  23.4 0.8 copy-done.1
  24.2 0.7 copy-done.2
  24.8 0.1 select_reduce_fusion.1
  25.0 0.1 iota_add_fusion
  25.0 0.1 broadcast_compare_fusion
  25.1 0.1 select_reduce_fusion
  25.3 0.2 fusion
  25.5 0.1 reshape.190
  25.6 0.3 broadcast_in_dim.78
  25.9 0.1 reshape.189
  26.1 0.7 and_select_fusion.1.bias_ref
  26.8 0.1 broadcast_compare_fusion.1
  26.9 0.1 compare_and_fusion
  27.0 0.7 and_select_fusion.pbias_ref
  27.7 47.9 %shard_map.92 = bf16[4,32,4096]{2,1,0:T(8,128)(2,1)} custom-call(bf16[4,128,512]{2,1,0:T(8,128)(2,1)} %copy-done.1, bf16[4,144,1024]{2,1,0:T(8,128)(2,1)} %copy-done, f32[4,128,16]{2,1,0:T(8,128)} %copy-done.2, f32[4,4,16,128]{3,2,1,0:T(8,128)} %and_select_fusion.1.bias_ref, f32[4,128,64]{2,1,0:T(8,128)} %and_select_fusion.pbias_ref, bf16[2048,1024]{1,0:T(8,128)(2,1)} %w_hbm.1), custom_call_target="tpu_custom_call" | custom-call | tf_op jit(solution)/shard_map/pallas_call | solution.py:417
  75.6 0.7 fusion.6
  83.9 1.3 %dynamic-slice_bitcast_fusion.3 = (bf16[32,1,4096]{2,0,1:T(8,128)(2,1)S(1)}, bf16[32,1,4096]{2,0,1:T(8,128)(2,1)S(1)}, bf16[32,1,4096]{2,0,1:T(8,128)(2,1)S(1)}, bf16[32,1,4096]{2,0,1:T(8,128)(2,1)S(1)}) fusion(bf16[4,32,4096]{2,1,0:T(8,128)(2,1)} %shard_map.92, s32[]{:T(128)S(6)} %select_n.64, s32[]{:T(128)S(6)} %select_n.67, s32[]{:T(128)S(6)} %select_n.66, ...), kind=kLoop, calls=%fused_computation.4 | loop fusion | bytes 2097168 | tf_op jit(solution)/shard_map/stack | solution.py:444
  85.2 0.1 pad_maximum_fusion
  85.3 1.8 %copy.22 = bf16[32,4,4096]{2,1,0:T(4,128)(2,1)} copy(bf16[32,4,4096]{2,0,1:T(8,128)(2,1)S(1)} %pad_maximum_fusion) | data formatting | bytes 2097152 | tf_op jit(solution)/shard_map/stack | solution.py:444
  (15 shorter events, 0.1 us)
Async XLA Ops:
  1.9 6.5 %copy-start.4 = (bf16[4096,2,8]{0,2,1:T(8,128)(2,1)S(1)}, bf16[4096,2,8]{0,2,1:T(8,128)(2,1)}, u32[]{:S(2)}) copy-start(bf16[4096,2,8]{0,2,1:T(8,128)(2,1)} %param.15) | copy-start | bytes 393220
  1.9 7.0 %copy-start.3 = (s32[4]{0:T(128)S(1)}, s32[4]{0:T(128)}, u32[]{:S(2)}) copy-start(s32[4]{0:T(128)} %len_ref.1) | copy-start | bytes 52
  8.9 16.2 %copy-start.5 = (s32[4,8,2,8]{3,2,1,0:T(2,128)S(1)}, s32[4,8,2,8]{3,2,1,0:T(2,128)}, u32[]{:S(2)}) copy-start(s32[4,8,2,8]{3,2,1,0:T(2,128)} %param.11) | copy-start | bytes 6148
  22.3 1.0 %copy-start = (bf16[4,144,1024]{2,1,0:T(8,128)(2,1)}, bf16[4,144,1024]{2,1,0:T(8,128)(2,1)S(1)}, u32[]{:S(2)}) copy-start(bf16[4,144,1024]{2,1,0:T(8,128)(2,1)S(1)} %get-tuple-element.9.kv_ref) | copy-start | bytes 3538948
  23.4 0.8 copy-start.1
  24.1 0.7 copy-start.2

commit v2 on v1

--- a/solution.py
+++ b/solution.py
@@ -26,53 +26,16 @@
     return slots
 
 
-def project_kernel(
-    rank_ref, len_ref, base_ref, x_ref, wq_ref, wk_ref, wv_ref, wg_ref, pool_ref,
-    q_ref, kv_ref, g_ref, acc, gacc,
-):
-    step = pl.program_id(0)
-    width = wq_ref.shape[1]
-    x = x_ref[...]
-
-    @pl.when(step == 0)
-    def _():
-        acc[...] = jnp.zeros_like(acc)
-        gacc[...] = jnp.zeros_like(gacc)
-
-    for n, w in enumerate((wq_ref, wk_ref, wv_ref)):
-        acc[:, n * width : (n + 1) * width] += jnp.dot(
-            x, w[...], preferred_element_type=jnp.float32
-        )
-    gacc[...] += jnp.dot(x, wg_ref[...], preferred_element_type=jnp.float32)
-
-    @pl.when(step == pl.num_programs(0) - 1)
-    def _():
-        seqs, rows, _ = q_ref.shape
-        pool = pool_ref[...]
-        for s in range(seqs):
-            at = rank_ref[s]
-            span = slice(s * rows, (s + 1) * rows)
-            q = acc[span, :width].astype(jnp.bfloat16)
-            q_ref[at] = q * jnp.bfloat16(HD**-0.5)
-            kv = acc[span, width:].astype(jnp.bfloat16)
-            kv_ref[at, :rows, :] = kv
-            grouped = kv.astype(jnp.float32).reshape(rows // L_CMP, L_CMP, 2 * width)
-            pooled = (grouped * pool[None]).sum(1)
-            fill = jnp.zeros((PAD - rows // L_CMP, 2 * width), jnp.float32)
-            kv_ref[at, rows:, :] = jnp.concatenate([pooled, fill], 0).astype(jnp.bfloat16)
-            gate = jax.nn.sigmoid(gacc[span, :])
-            pos = base_ref[0] + lax.broadcasted_iota(jnp.int32, gate.shape, 0)
-            g_ref[at] = jnp.where(pos < len_ref[s], gate, 0.0)
-
-
 def mixer_kernel(
     slots, shards, ntp,
-    q_ref, kv_ref, g_ref, bias_ref, pbias_ref, w_hbm,
-    out_ref,
-    items, att, mixed, pools, acc, top, tot, w_vmem,
-    w_sem, z_send, z_recv, a_send, a_recv, o_send, o_recv,
+    len_ref, chosen_ref, pool_ref, wg_ref, tok_hbm, wq_hbm, wk_hbm, wv_hbm, w_hbm,
+    final_ref,
+    tok, xt, proj, q_ref, kv_ref, g_ref, out_ref,
+    items, att, mixed, pools, acc, top, tot, wq_vmem, wk_vmem, wv_vmem, w_vmem,
+    in_sem, q_sem, w_sem, z_send, z_recv, a_send, a_recv, o_send, o_recv,
 ):
     seqs, rows, width = q_ref.shape
+    steps, _, _, depth = tok.shape
     heads = width // HD
     pairs = heads // 2
     blocks = rows // QB
@@ -84,9 +47,46 @@
     x, c = t // 2, t % 2
     mate = x * 2 + (1 - c)
 
+    def span_of(k):
+        return pl.ds(pl.multiple_of(k * depth, depth), depth)
+
+    def input_copies(k):
+        return (
+            pltpu.make_async_copy(tok_hbm.at[:, :, span_of(k)], tok.at[k], in_sem.at[k, 0]),
+            pltpu.make_async_copy(wk_hbm.at[span_of(k)], wk_vmem.at[span_of(k)], in_sem.at[k, 1]),
+            pltpu.make_async_copy(wv_hbm.at[span_of(k)], wv_vmem.at[span_of(k)], in_sem.at[k, 2]),
+        )
+
+    for k in range(steps):
+        for copy in input_copies(k):
+            copy.start()
+    q_copy = pltpu.make_async_copy(wq_hbm, wq_vmem, q_sem)
+    q_copy.start()
     w_copy = pltpu.make_async_copy(w_hbm, w_vmem, w_sem)
     w_copy.start()
     pools[...] = jnp.zeros_like(pools)
+
+    lens = [len_ref[s] for s in range(seqs)]
+    ranks = []
+    for s in range(seqs):
+        place = jnp.int32(0)
+        for o in range(seqs):
+            if o != s:
+                ahead = lens[o] >= lens[s] if o < s else lens[o] > lens[s]
+                place = place + jnp.where(ahead, 1, 0)
+        ranks.append(place)
+
+    def seq_at(r):
+        found = jnp.int32(0)
+        for s in range(1, seqs):
+            found = found + jnp.where(ranks[s] == r, s, 0)
+        return found
+
+    def live_at(r):
+        found = jnp.int32(0)
+        for s in range(seqs):
+            found = found + jnp.where(ranks[s] == r, lens[s], 0)
+        return found
 
     def active(shard):
         count = 0
@@ -111,6 +111,33 @@
     def _():
         pl.semaphore_signal(barrier, inc=1, device_id={"kv": i + 1}, device_id_type=MESH)
 
+    def project(k, carry):
+        for copy in input_copies(k):
+            copy.wait()
+        piece = jnp.swapaxes(tok[k], 0, 1).reshape(seqs * rows, depth)
+        xt[k] = piece
+        for n, w in enumerate((wk_vmem, wv_vmem)):
+            product = jnp.dot(piece, w[span_of(k), :], preferred_element_type=jnp.float32)
+            product = product.reshape(seqs, rows, width)
+            span = slice(n * width, (n + 1) * width)
+
+            @pl.when(k == 0)
+            def _():
+                proj[:, :, span] = product
+
+            @pl.when(k > 0)
+            def _():
+                proj[:, :, span] += product
+
+        return carry
+
+    lax.fori_loop(0, steps, project, 0)
+
+    def keep(r, carry):
+        kv_ref[r] = proj[seq_at(r)].astype(jnp.bfloat16)
+        return carry
+
+    lax.fori_loop(0, seqs, keep, 0)
     expected = ntp - 1 + jnp.where(i > 0, 1, 0) + jnp.where(i < shards - 1, 1, 0)
     pl.semaphore_wait(barrier, expected)
 
@@ -154,7 +181,37 @@
         own_copy(r).start()
         return carry
 
-    lax.fori_loop(0, after, send_own, 0)
+    lax.fori_loop(0, jnp.where(i == 0, after, jnp.minimum(after, 1)), send_own, 0)
+
+    q_copy.wait()
+
+    def project_queries(k, carry):
+        piece = xt[k]
+        product = jnp.dot(piece, wq_vmem[span_of(k), :], preferred_element_type=jnp.float32)
+        product = product.reshape(seqs, rows, width)
+        gate = lax.dot_general(piece, wg_ref[k], NT, preferred_element_type=jnp.float32)
+        gate = gate.reshape(seqs, rows, 2 * heads)
+
+        @pl.when(k == 0)
+        def _():
+            proj[:, :, :width] = product
+            g_ref[...] = gate
+
+        @pl.when(k > 0)
+        def _():
+            proj[:, :, :width] += product
+            g_ref[...] += gate
+
+        return carry
+
+    lax.fori_loop(0, steps, project_queries, 0)
+    g_ref[...] = jax.nn.sigmoid(g_ref[...])
+
+    def keep_queries(r, carry):
+        q_ref[r] = proj[seq_at(r), :, :width].astype(jnp.bfloat16) * jnp.bfloat16(HD**-0.5)
+        return carry
+
+    lax.fori_loop(0, mine, keep_queries, 0)
 
     lane = lax.broadcasted_iota(jnp.int32, (rows, 2 * HD), 1)
     first = lane < HD
@@ -170,12 +227,29 @@
         )
         return scores + bias
 
-    def block_bias(r, j, p):
+    def chunk_bias(r, j):
+        listed = chosen_ref[seq_at(r)]
+        key_at = j * rows + lax.broadcasted_iota(jnp.int32, (heads * blocks, rows), 1)
+        key_blk = key_at // QB
+        hit = listed[:, :1] == key_blk
+        for n in range(1, listed.shape[1]):
+            hit = hit | (listed[:, n : n + 1] == key_blk)
+        return jnp.where(hit & (key_at < live_at(r)), 0.0, LOW)
+
+    def block_bias(bias, p):
         lines = [
-            jnp.broadcast_to(bias_ref[r, j, n : n + 1, :], (QB, rows))
+            jnp.broadcast_to(bias[n : n + 1, :], (QB, rows))
             for n in range(p * 2 * blocks, (p + 1) * 2 * blocks)
         ]
         return jnp.concatenate(lines, 0)
+
+    def pool_rows(kv, j):
+        grouped = kv.astype(jnp.float32).reshape(rows // L_CMP, L_CMP, 2 * width)
+        pooled = (grouped * pool_ref[...][None]).sum(1)
+        fill = jnp.zeros((PAD - rows // L_CMP, 2 * width), jnp.float32)
+        pools[pl.ds(pl.multiple_of(j * PAD, PAD), PAD), :] = jnp.concatenate(
+            [pooled, fill], 0
+        ).astype(jnp.bfloat16)
 
     def columns(p):
         return slice(p * 2 * HD, (p + 1) * 2 * HD)
@@ -188,9 +262,10 @@
         row = jnp.where(row >= rows, row - rows, row)
         key = lax.broadcasted_iota(jnp.int32, (2 * rows, rows), 1)
         causal = jnp.where(key <= row, 0.0, LOW)
-        pools[pl.ds(pl.multiple_of(i * PAD, PAD), PAD), :] = kv_ref[r, rows:, :]
+        pool_rows(kv_ref[r], i)
+        own_bias = chunk_bias(r, i)
         for p in range(pairs):
-            bias = block_bias(r, i, p) + causal
+            bias = block_bias(own_bias, p) + causal
             scores = scores_of(r, p, kv_ref[r, :rows, columns(p)], bias)
             peak = jnp.maximum(jnp.max(scores, axis=1, keepdims=True), FLOOR)
             e = jnp.exp(scores - peak)
@@ -202,10 +277,11 @@
             )
 
         def chunk(j, carry):
-            pools[pl.ds(pl.multiple_of(j * PAD, PAD), PAD), :] = items[r, j, rows:, :]
+            pool_rows(items[r, j], j)
+            bias = chunk_bias(r, j)
             for p in range(pairs):
                 scores = scores_of(
-                    r, p, items[r, j, :rows, columns(p)], block_bias(r, j, p)
+                    r, p, items[r, j, :rows, columns(p)], block_bias(bias, p)
                 )
                 old = top[p]
                 peak = jnp.maximum(old, jnp.max(scores, axis=1, keepdims=True))
@@ -221,8 +297,17 @@
 
         lax.fori_loop(0, i, chunk, 0)
 
-        pbias = pbias_ref[r]
+        pshape = (rows, shards * PAD)
+        pslot = lax.broadcasted_iota(jnp.int32, pshape, 1)
+        inner = pslot % PAD
+        end = (pslot // PAD) * rows + inner * L_CMP + L_CMP - 1
+        pos = i * rows + lax.broadcasted_iota(jnp.int32, pshape, 0)
+        usable = (inner < rows // L_CMP) & (end <= pos) & (end < live_at(r))
+        pbias = jnp.where(usable, 0.0, LOW)
         pbias = jnp.concatenate([pbias, pbias], 0)
+        gates = g_ref[seq_at(r)]
+        gate_pos = i * rows + lax.broadcasted_iota(jnp.int32, gates.shape, 0)
+        gates = jnp.where(gate_pos < live_at(r), gates, 0.0)
         for p in range(pairs):
             scores = scores_of(r, p, pools[:, columns(p)], pbias)
             peak = jnp.maximum(jnp.max(scores, axis=1, keepdims=True), FLOOR)
@@ -239,8 +324,8 @@
                 h = 2 * p + side_at
                 span = slice(side_at * rows, (side_at + 1) * rows)
                 halves.append(
-                    g_ref[r, :, h : h + 1] * pooled[span]
-                    + g_ref[r, :, heads + h : heads + h + 1] * picked[span]
+                    gates[:, h : h + 1] * pooled[span]
+                    + gates[:, heads + h : heads + h + 1] * picked[span]
                 )
             att[r, t, :, columns(p)] = jnp.where(first, halves[0], halves[1]).astype(
                 jnp.bfloat16
@@ -260,6 +345,11 @@
                 return inner
 
             lax.fori_loop(0, i, arrive, 0)
+
+            @pl.when((i > 0) & (r + 1 < after))
+            def _():
+                own_copy(r + 1).start()
+
             attend(r)
             for d in range(1, chips):
                 block_copy(r, d, t, side(d)).start()
@@ -320,6 +410,9 @@
 
     lax.fori_loop(0, mine, finish, 0)
 
+    parts = jnp.stack([out_ref[ranks[s]] for s in range(seqs)], 0)
+    final_ref[...] = jnp.swapaxes(parts, 0, 1)
+
     def sent(r, carry):
         own_copy(r).wait_send()
 
@@ -340,94 +433,50 @@
     col = w_out.shape[1]
     shards = lax.axis_size("kv")
     ntp = lax.axis_size("tp")
-    shard = lax.axis_index("kv")
-    base = (shard * rows).astype(jnp.int32)
+    chips = ntp // 2
     blocks = rows // QB
     slots = rank_slots(seqs, rows * shards, rows, shards)
-
-    ids = jnp.arange(seqs)
-    ahead = (lengths[None, :] > lengths[:, None]) | (
-        (lengths[None, :] == lengths[:, None]) & (ids[None, :] < ids[:, None])
-    )
-    rank = jnp.sum(ahead.astype(jnp.int32), axis=1)
-    order = rank[None, :] == ids[:, None]
-    sorted_len = jnp.sum(jnp.where(order, lengths[None, :], 0), axis=1)
-    ranked = jnp.sum(jnp.where(order[:, :, None, None, None], chosen[None], 0), axis=1)
-
-    block_ids = jnp.arange(shards * blocks)
-    picked = jnp.any(ranked[..., None] == block_ids, axis=3)
-    picked = picked.reshape(seqs, heads * blocks, shards, blocks).transpose(0, 2, 1, 3)
-    picked = jnp.repeat(picked, QB, axis=3)
-    key_pos = (jnp.arange(shards) * rows)[:, None] + jnp.arange(rows)[None, :]
-    near = key_pos[None, :, None, :] < sorted_len[:, None, None, None]
-    bias = jnp.where(picked & near, 0.0, LOW).astype(jnp.float32)
-
-    slot = jnp.arange(shards * PAD)
-    inner = slot % PAD
-    end = (slot // PAD) * rows + inner * L_CMP + L_CMP - 1
-    pos = base + jnp.arange(rows)
-    usable = (
-        (inner < rows // L_CMP)[None, None, :]
-        & (end[None, None, :] <= pos[None, :, None])
-        & (end[None, None, :] < sorted_len[:, None, None])
-    )
-    pbias = jnp.where(usable, 0.0, LOW).astype(jnp.float32)
+    steps = 4
+    depth = model // steps
+
     pool = jnp.concatenate(
         [jnp.tile(pool_weights[0], (1, heads)), jnp.tile(pool_weights[1], (1, heads))], 1
     )
-
-    flat = tokens.transpose(1, 0, 2).reshape(seqs * rows, model)
-    gate_w = w_gate.reshape(model, 2 * heads)
-    depth = model // 8
-    whole = lambda k, *_: (0, 0)
-    q, kv, gates = pl.pallas_call(
-        project_kernel,
-        grid_spec=pltpu.PrefetchScalarGridSpec(
-            num_scalar_prefetch=3,
-            grid=(model // depth,),
-            in_specs=[
-                pl.BlockSpec((seqs * rows, depth), lambda k, *_: (0, k)),
-                pl.BlockSpec((depth, width), lambda k, *_: (k, 0)),
-                pl.BlockSpec((depth, width), lambda k, *_: (k, 0)),
-                pl.BlockSpec((depth, width), lambda k, *_: (k, 0)),
-                pl.BlockSpec((depth, 2 * heads), lambda k, *_: (k, 0)),
-                pl.BlockSpec((L_CMP, 2 * width), whole),
-            ],
-            out_specs=[
-                pl.BlockSpec((seqs, rows, width), lambda k, *_: (0, 0, 0)),
-                pl.BlockSpec((seqs, rows + PAD, 2 * width), lambda k, *_: (0, 0, 0)),
-                pl.BlockSpec((seqs, rows, 2 * heads), lambda k, *_: (0, 0, 0)),
-            ],
-            scratch_shapes=[
-                pltpu.VMEM((seqs * rows, 3 * width), jnp.float32),
-                pltpu.VMEM((seqs * rows, 2 * heads), jnp.float32),
-            ],
-        ),
-        out_shape=[
-            jax.ShapeDtypeStruct((seqs, rows, width), jnp.bfloat16),
-            jax.ShapeDtypeStruct((seqs, rows + PAD, 2 * width), jnp.bfloat16),
-            jax.ShapeDtypeStruct((seqs, rows, 2 * heads), jnp.float32),
-        ],
-        compiler_params=pltpu.CompilerParams(vmem_limit_bytes=48 * 2**20),
-    )(rank, lengths, base[None], flat, w_query, w_key, w_value, gate_w, pool)
-
-    chips = ntp // 2
+    listed = chosen.reshape(seqs, heads * blocks, chosen.shape[3])
+    gate_w = w_gate.transpose(1, 2, 0).reshape(2 * heads, steps, depth).transpose(1, 0, 2)
+
     vmem = pl.BlockSpec(memory_space=pltpu.VMEM)
+    smem = pl.BlockSpec(memory_space=pltpu.SMEM)
+    anywhere = pl.BlockSpec(memory_space=pl.ANY)
     dma = pltpu.SemaphoreType.DMA
-    out = pl.pallas_call(
+    bf16, f32 = jnp.bfloat16, jnp.float32
+    state = pltpu.VMEM((heads // 2, 2 * rows, 2 * HD), f32)
+    return pl.pallas_call(
         functools.partial(mixer_kernel, slots, shards, ntp),
-        out_shape=jax.ShapeDtypeStruct((seqs, rows // ntp, ntp * col), jnp.bfloat16),
-        in_specs=[vmem] * 5 + [pl.BlockSpec(memory_space=pl.ANY)],
+        out_shape=jax.ShapeDtypeStruct((rows // ntp, seqs, ntp * col), bf16),
+        in_specs=[smem] + [vmem] * 3 + [anywhere] * 5,
         out_specs=vmem,
         scratch_shapes=[
-            pltpu.VMEM((seqs, shards, rows + PAD, 2 * width), jnp.bfloat16),
-            pltpu.VMEM((seqs, ntp, rows, width), jnp.bfloat16),
-            pltpu.VMEM((seqs, rows, col), jnp.bfloat16),
-            pltpu.VMEM((shards * PAD, 2 * width), jnp.bfloat16),
-            pltpu.VMEM((heads // 2, 2 * rows, 2 * HD), jnp.float32),
-            pltpu.VMEM((heads // 2, 2 * rows, 2 * HD), jnp.float32),
-            pltpu.VMEM((heads // 2, 2 * rows, 2 * HD), jnp.float32),
-            pltpu.VMEM(w_out.shape, jnp.bfloat16),
+            pltpu.VMEM((steps, rows, seqs, depth), bf16),
+            pltpu.VMEM((steps, seqs * rows, depth), bf16),
+            pltpu.VMEM((seqs, rows, 2 * width), f32),
+            pltpu.VMEM((seqs, rows, width), bf16),
+            pltpu.VMEM((seqs, rows, 2 * width), bf16),
+            pltpu.VMEM((seqs, rows, 2 * heads), f32),
+            pltpu.VMEM((seqs, rows // ntp, ntp * col), bf16),
+            pltpu.VMEM((seqs, shards, rows, 2 * width), bf16),
+            pltpu.VMEM((seqs, ntp, rows, width), bf16),
+            pltpu.VMEM((seqs, rows, col), bf16),
+            pltpu.VMEM((shards * PAD, 2 * width), bf16),
+            state,
+            state,
+            state,
+            pltpu.VMEM(w_query.shape, bf16),
+            pltpu.VMEM(w_key.shape, bf16),
+            pltpu.VMEM(w_value.shape, bf16),
+            pltpu.VMEM(w_out.shape, bf16),
+            dma((steps, 3)),
+            dma,
             dma,
             dma((seqs, shards)),
             dma((seqs, shards)),
@@ -437,11 +486,9 @@
             dma((seqs, ntp)),
         ],
         compiler_params=pltpu.CompilerParams(
-            collective_id=0, has_side_effects=True, vmem_limit_bytes=56 * 2**20
+            collective_id=0, has_side_effects=True, vmem_limit_bytes=60 * 2**20
         ),
-    )(q, kv, gates, bias, pbias, w_out)
-    parts = [lax.dynamic_index_in_dim(out, rank[s], 0, keepdims=False) for s in range(seqs)]
-    return jnp.stack(parts, axis=1)
+    )(lengths, listed, pool, gate_w, tokens, w_query, w_key, w_value, w_out)
 
 
 def solution(mesh):

time: 87.6 us -> 57.1 us (0.65)
  the two profiles are of different devices: /device:TPU:25 before, /device:TPU:17 now
where the time goes in v2:
time: 57.1 us; the launch traced here: 56.7 us
  Pallas kernels  50.6 us (89%)
  local copies, waits for them, and re-layouts  5.44 us (10%)
  other arithmetic  0.66 us (1%)
    pallas_call x1, Pallas kernels, body(): pl.pallas_call(functools.partial(mixer_kernel, slots, shards, ntp), out_s...  50.6 us
    unnamed x1, local copies, waits for them, and re-layouts  2.82 us
    reshape x2, local copies, waits for them, and re-layouts, body(): w_gate.transpose(1, 2, 0).reshape(2 * heads, steps, depth)  1.67 us

profile of v2, /device:TPU:17, one launch (start us, length us, event | category | flops | bytes accessed | tf_op | source)
XLA Modules:
  0.0 56.7 jit_solution(17705716565928591375)
XLA Ops:
  0.0 0.7 %slice_bitcast_fusion.1 = (f32[32,64]{1,0:T(8,128)S(1)}, f32[32,64]{1,0:T(8,128)S(1)}) fusion(f32[2,32,64]{2,1,0:T(8,128)} %param.16), kind=kLoop, calls=%fused_computation.3 | loop fusion | bytes 32768 | tf_op jit(solution)/shard_map/tile | solution.py:443
  0.8 0.1 tile.22
  0.9 0.1 tile.25
  1.0 0.7 %pad_maximum_fusion.pool_ref = f32[32,1024]{1,0:T(8,128)} fusion(f32[32,512]{1,0:T(8,128)S(1)} %tile.25, f32[32,512]{1,0:T(8,128)S(1)} %tile.22), kind=kLoop, calls=%fused_computation | loop fusion | flops 32768 | bytes 262144 | tf_op jit(solution)/shard_map/concatenate | solution.py:442
  1.6 1.0 %reshape.15 = bf16[16,4,1024]{2,1,0:T(4,128)(2,1)S(1)} reshape(bf16[2,8,4096]{2,1,0:T(8,128)(2,1)} %bitcast.10) | data formatting | bytes 262144 | tf_op jit(solution)/shard_map/reshape | solution.py:446
  2.6 0.7 %copy.12 = bf16[16,4,1024]{2,0,1:T(8,128)(2,1)} copy(bf16[16,4,1024]{2,1,0:T(4,128)(2,1)S(1)} %reshape.15) | data formatting | bytes 262144 | tf_op jit(solution)/shard_map/reshape | solution.py:446
  3.3 50.6 %shard_map.91 = bf16[32,4,4096]{2,1,0:T(4,128)(2,1)} custom-call(s32[4]{0:T(128)} %len_ref.1, s32[4,16,8]{2,1,0:T(8,128)} %bitcast.11, f32[32,1024]{1,0:T(8,128)} %pad_maximum_fusion.pool_ref, bf16[4,16,1024]{2,1,0:T(8,128)(2,1)} %bitcast.9, bf16[128,4,4096]{2,1,0:T(4,128)(2,1)} %tok_hbm.1, bf16[4096,512]{1,0:T(8,128)(2,1)} %wq_hbm.1, ...), custom_call_target="tpu_custom_call" | custom-call | tf_op jit(solution)/shard_map/pallas_call | solution.py:454
  53.9 2.8 %copy.14 = bf16[32,4,4096]{2,1,0:T(4,128)(2,1)} copy(bf16[32,4,4096]{2,1,0:T(4,128)(2,1)} %shard_map.91) | data formatting | bytes 2097152
  (2 shorter events, 0.0 us)

commit v3 on v2

--- a/solution.py
+++ b/solution.py
@@ -26,13 +26,32 @@
     return slots
 
 
+def ranks_of(lens):
+    ranks = []
+    for s in range(len(lens)):
+        place = jnp.int32(0)
+        for o in range(len(lens)):
+            if o != s:
+                ahead = lens[o] >= lens[s] if o < s else lens[o] > lens[s]
+                place = place + jnp.where(ahead, 1, 0)
+        ranks.append(place)
+    return ranks
+
+
+def order_kernel(len_ref, ranked_ref, out_ref):
+    seqs = ranked_ref.shape[0]
+    ranks = ranks_of([len_ref[s] for s in range(seqs)])
+    parts = jnp.stack([ranked_ref[ranks[s]] for s in range(seqs)], 0)
+    out_ref[...] = jnp.swapaxes(parts, 0, 1)
+
+
 def mixer_kernel(
     slots, shards, ntp,
-    len_ref, chosen_ref, pool_ref, wg_ref, tok_hbm, wq_hbm, wk_hbm, wv_hbm, w_hbm,
-    final_ref,
-    tok, xt, proj, q_ref, kv_ref, g_ref, out_ref,
+    len_ref, chosen_ref, pool_in, tok_hbm, wq_hbm, wk_hbm, wv_hbm, wg_hbm, w_hbm,
+    out_ref,
+    tok, xt, proj, q_ref, kv_ref, g_ref, pool_ref, wg_ref,
     items, att, mixed, pools, acc, top, tot, wq_vmem, wk_vmem, wv_vmem, w_vmem,
-    in_sem, q_sem, w_sem, z_send, z_recv, a_send, a_recv, o_send, o_recv,
+    in_sem, v_sem, q_sem, g_sem, w_sem, z_send, z_recv, a_send, a_recv, o_send, o_recv,
 ):
     seqs, rows, width = q_ref.shape
     steps, _, _, depth = tok.shape
@@ -54,27 +73,25 @@
         return (
             pltpu.make_async_copy(tok_hbm.at[:, :, span_of(k)], tok.at[k], in_sem.at[k, 0]),
             pltpu.make_async_copy(wk_hbm.at[span_of(k)], wk_vmem.at[span_of(k)], in_sem.at[k, 1]),
-            pltpu.make_async_copy(wv_hbm.at[span_of(k)], wv_vmem.at[span_of(k)], in_sem.at[k, 2]),
         )
 
     for k in range(steps):
         for copy in input_copies(k):
             copy.start()
+    v_copy = pltpu.make_async_copy(wv_hbm, wv_vmem, v_sem)
+    v_copy.start()
+    g_copy = pltpu.make_async_copy(wg_hbm, wg_ref, g_sem)
+    g_copy.start()
     q_copy = pltpu.make_async_copy(wq_hbm, wq_vmem, q_sem)
     q_copy.start()
     w_copy = pltpu.make_async_copy(w_hbm, w_vmem, w_sem)
     w_copy.start()
     pools[...] = jnp.zeros_like(pools)
+    for n in range(2):
+        pool_ref[:, n * width : (n + 1) * width] = jnp.concatenate([pool_in[n]] * heads, 1)
 
     lens = [len_ref[s] for s in range(seqs)]
-    ranks = []
-    for s in range(seqs):
-        place = jnp.int32(0)
-        for o in range(seqs):
-            if o != s:
-                ahead = lens[o] >= lens[s] if o < s else lens[o] > lens[s]
-                place = place + jnp.where(ahead, 1, 0)
-        ranks.append(place)
+    ranks = ranks_of(lens)
 
     def seq_at(r):
         found = jnp.int32(0)
@@ -116,42 +133,50 @@
             copy.wait()
         piece = jnp.swapaxes(tok[k], 0, 1).reshape(seqs * rows, depth)
         xt[k] = piece
-        for n, w in enumerate((wk_vmem, wv_vmem)):
-            product = jnp.dot(piece, w[span_of(k), :], preferred_element_type=jnp.float32)
-            product = product.reshape(seqs, rows, width)
-            span = slice(n * width, (n + 1) * width)
-
-            @pl.when(k == 0)
-            def _():
-                proj[:, :, span] = product
-
-            @pl.when(k > 0)
-            def _():
-                proj[:, :, span] += product
-
-        return carry
+        accumulate(k, piece, wk_vmem, 0)
+        return carry
+
+    def accumulate(k, piece, w, n):
+        product = jnp.dot(piece, w[span_of(k), :], preferred_element_type=jnp.float32)
+        product = product.reshape(seqs, rows, width)
+        span = slice(n * width, (n + 1) * width)
+
+        @pl.when(k == 0)
+        def _():
+            proj[:, :, span] = product
+
+        @pl.when(k > 0)
+        def _():
+            proj[:, :, span] += product
+
+    def keep(n):
+        span = slice(n * width, (n + 1) * width)
+
+        def one(r, carry):
+            kv_ref[r, :, span] = proj[seq_at(r), :, span].astype(jnp.bfloat16)
+            return carry
+
+        lax.fori_loop(0, seqs, one, 0)
 
     lax.fori_loop(0, steps, project, 0)
-
-    def keep(r, carry):
-        kv_ref[r] = proj[seq_at(r)].astype(jnp.bfloat16)
-        return carry
-
-    lax.fori_loop(0, seqs, keep, 0)
+    keep(0)
     expected = ntp - 1 + jnp.where(i > 0, 1, 0) + jnp.where(i < shards - 1, 1, 0)
     pl.semaphore_wait(barrier, expected)
 
-    def own_copy(r):
+    def half(n):
+        return slice(n * width, (n + 1) * width)
+
+    def own_copy(r, n):
         return pltpu.make_async_remote_copy(
-            src_ref=kv_ref.at[r], dst_ref=items.at[r, i],
-            send_sem=z_send.at[r, i], recv_sem=z_recv.at[r, i],
+            src_ref=kv_ref.at[r, :, half(n)], dst_ref=items.at[r, i, :, half(n)],
+            send_sem=z_send.at[r, i, n], recv_sem=z_recv.at[r, i, n],
             device_id={"kv": i + 1}, device_id_type=MESH,
         )
 
-    def relay_copy(r, j):
+    def relay_copy(r, j, n):
         return pltpu.make_async_remote_copy(
-            src_ref=items.at[r, j], dst_ref=items.at[r, j],
-            send_sem=z_send.at[r, j], recv_sem=z_recv.at[r, j],
+            src_ref=items.at[r, j, :, half(n)], dst_ref=items.at[r, j, :, half(n)],
+            send_sem=z_send.at[r, j, n], recv_sem=z_recv.at[r, j, n],
             device_id={"kv": i + 1}, device_id_type=MESH,
         )
 
@@ -177,19 +202,46 @@
             device_id={"tp": target}, device_id_type=MESH,
         )
 
+    @pl.when(after > 0)
+    def _():
+        own_copy(0, 0).start()
+
+    @pl.when((i == 0) & (after > 1))
+    def _():
+        own_copy(1, 0).start()
+
+    v_copy.wait()
+
+    def project_values(k, carry):
+        accumulate(k, xt[k], wv_vmem, 1)
+        return carry
+
+    lax.fori_loop(0, steps, project_values, 0)
+    keep(1)
+
+    @pl.when(after > 0)
+    def _():
+        own_copy(0, 1).start()
+
+    @pl.when((i == 0) & (after > 1))
+    def _():
+        own_copy(1, 1).start()
+
     def send_own(r, carry):
-        own_copy(r).start()
-        return carry
-
-    lax.fori_loop(0, jnp.where(i == 0, after, jnp.minimum(after, 1)), send_own, 0)
-
+        own_copy(r, 0).start()
+        own_copy(r, 1).start()
+        return carry
+
+    lax.fori_loop(2, jnp.where(i == 0, after, 2), send_own, 0)
+
+    g_copy.wait()
     q_copy.wait()
 
     def project_queries(k, carry):
         piece = xt[k]
         product = jnp.dot(piece, wq_vmem[span_of(k), :], preferred_element_type=jnp.float32)
         product = product.reshape(seqs, rows, width)
-        gate = lax.dot_general(piece, wg_ref[k], NT, preferred_element_type=jnp.float32)
+        gate = jnp.dot(piece, wg_ref[span_of(k), :], preferred_element_type=jnp.float32)
         gate = gate.reshape(seqs, rows, 2 * heads)
 
         @pl.when(k == 0)
@@ -257,7 +309,7 @@
     def value_columns(p):
         return slice(width + p * 2 * HD, width + (p + 1) * 2 * HD)
 
-    def attend(r):
+    def attend_own(r):
         row = lax.broadcasted_iota(jnp.int32, (2 * rows, rows), 0)
         row = jnp.where(row >= rows, row - rows, row)
         key = lax.broadcasted_iota(jnp.int32, (2 * rows, rows), 1)
@@ -276,6 +328,7 @@
                 preferred_element_type=jnp.float32,
             )
 
+    def attend(r):
         def chunk(j, carry):
             pool_rows(items[r, j], j)
             bias = chunk_bias(r, j)
@@ -334,13 +387,16 @@
     def step(r, carry):
         @pl.when(r < mine)
         def _():
-            def arrive(n, inner):
-                j = i - 1 - n
-                relay_copy(r, j).wait_recv()
-
-                @pl.when(r < after)
-                def _():
-                    relay_copy(r, j).start()
+            attend_own(r)
+
+            def arrive(m, inner):
+                j = i - 1 - m
+                for n in range(2):
+                    relay_copy(r, j, n).wait_recv()
+
+                    @pl.when(r < after)
+                    def _():
+                        relay_copy(r, j, n).start()
 
                 return inner
 
@@ -348,7 +404,8 @@
 
             @pl.when((i > 0) & (r + 1 < after))
             def _():
-                own_copy(r + 1).start()
+                own_copy(r + 1, 0).start()
+                own_copy(r + 1, 1).start()
 
             attend(r)
             for d in range(1, chips):
@@ -410,14 +467,13 @@
 
     lax.fori_loop(0, mine, finish, 0)
 
-    parts = jnp.stack([out_ref[ranks[s]] for s in range(seqs)], 0)
-    final_ref[...] = jnp.swapaxes(parts, 0, 1)
-
     def sent(r, carry):
-        own_copy(r).wait_send()
+        for n in range(2):
+            own_copy(r, n).wait_send()
 
         def relayed(j, inner):
-            relay_copy(r, j).wait_send()
+            for n in range(2):
+                relay_copy(r, j, n).wait_send()
             return inner
 
         lax.fori_loop(0, i, relayed, 0)
@@ -439,11 +495,8 @@
     steps = 4
     depth = model // steps
 
-    pool = jnp.concatenate(
-        [jnp.tile(pool_weights[0], (1, heads)), jnp.tile(pool_weights[1], (1, heads))], 1
-    )
     listed = chosen.reshape(seqs, heads * blocks, chosen.shape[3])
-    gate_w = w_gate.transpose(1, 2, 0).reshape(2 * heads, steps, depth).transpose(1, 0, 2)
+    gate_w = w_gate.reshape(model, 2 * heads)
 
     vmem = pl.BlockSpec(memory_space=pltpu.VMEM)
     smem = pl.BlockSpec(memory_space=pltpu.SMEM)
@@ -451,10 +504,10 @@
     dma = pltpu.SemaphoreType.DMA
     bf16, f32 = jnp.bfloat16, jnp.float32
     state = pltpu.VMEM((heads // 2, 2 * rows, 2 * HD), f32)
-    return pl.pallas_call(
+    ranked = pl.pallas_call(
         functools.partial(mixer_kernel, slots, shards, ntp),
-        out_shape=jax.ShapeDtypeStruct((rows // ntp, seqs, ntp * col), bf16),
-        in_specs=[smem] + [vmem] * 3 + [anywhere] * 5,
+        out_shape=jax.ShapeDtypeStruct((seqs, rows // ntp, ntp * col), bf16),
+        in_specs=[smem] + [vmem] * 2 + [anywhere] * 6,
         out_specs=vmem,
         scratch_shapes=[
             pltpu.VMEM((steps, rows, seqs, depth), bf16),
@@ -463,7 +516,8 @@
             pltpu.VMEM((seqs, rows, width), bf16),
             pltpu.VMEM((seqs, rows, 2 * width), bf16),
             pltpu.VMEM((seqs, rows, 2 * heads), f32),
-            pltpu.VMEM((seqs, rows // ntp, ntp * col), bf16),
+            pltpu.VMEM((L_CMP, 2 * width), f32),
+            pltpu.VMEM((model, 2 * heads), bf16),
             pltpu.VMEM((seqs, shards, rows, 2 * width), bf16),
             pltpu.VMEM((seqs, ntp, rows, width), bf16),
             pltpu.VMEM((seqs, rows, col), bf16),
@@ -475,11 +529,13 @@
             pltpu.VMEM(w_key.shape, bf16),
             pltpu.VMEM(w_value.shape, bf16),
             pltpu.VMEM(w_out.shape, bf16),
-            dma((steps, 3)),
+            dma((steps, 2)),
             dma,
             dma,
-            dma((seqs, shards)),
-            dma((seqs, shards)),
+            dma,
+            dma,
+            dma((seqs, shards, 2)),
+            dma((seqs, shards, 2)),
             dma((seqs, 2 * chips)),
             dma((seqs, 2 * chips)),
             dma((seqs, ntp)),
@@ -488,7 +544,19 @@
         compiler_params=pltpu.CompilerParams(
             collective_id=0, has_side_effects=True, vmem_limit_bytes=60 * 2**20
         ),
-    )(lengths, listed, pool, gate_w, tokens, w_query, w_key, w_value, w_out)
+    )(lengths, listed, pool_weights, tokens, w_query, w_key, w_value, gate_w, w_out)
+    part = rows // ntp
+    tile = ntp * col // 4
+    return pl.pallas_call(
+        order_kernel,
+        grid_spec=pltpu.PrefetchScalarGridSpec(
+            num_scalar_prefetch=1,
+            grid=(4,),
+            in_specs=[pl.BlockSpec((seqs, part, tile), lambda k, *_: (0, 0, k))],
+            out_specs=pl.BlockSpec((part, seqs, tile), lambda k, *_: (0, 0, k)),
+        ),
+        out_shape=jax.ShapeDtypeStruct((part, seqs, ntp * col), bf16),
+    )(lengths, ranked)
 
 
 def solution(mesh):

time: 57.1 us -> 55 us (0.963)
  local copies, waits for them, and re-layouts: 5.44 us -> 2.22 us
  Pallas kernels: 50.6 us -> 52.5 us
  other arithmetic: 0.66 us -> 0 us
    pallas_call x0 -> x1, Pallas kernels: none -> 4.1 us  [body(): pl.pallas_call(order_kernel, grid_spec=pltpu.PrefetchScalarGridSpec(num_s...]
    unnamed x1 -> x0, local copies, waits for them, and re-layouts: 2.82 us -> none
    pallas_call x1, Pallas kernels: 50.6 us -> 48.4 us  [body(): pl.pallas_call(functools.partial(mixer_kernel, slots, shards, ntp), out_s...]
    another operation x5 -> x0, local copies, waits for them, and re-layouts: 0.94 us -> none  [the longest x3 0.84 us: body(): jnp.tile(pool_weights[0], (1, heads))]
    concatenate x1 -> x0, other arithmetic: 0.66 us -> none  [body(): jnp.concatenate([jnp.tile(pool_weights[0], (1, heads)), jnp.tile(pool_wei...]
    reshape x2 -> x1, local copies, waits for them, and re-layouts: 1.67 us -> 2.22 us  [body(): gate_w = w_gate.reshape(model, 2 * heads)]
where the time goes in v3:
time: 55 us; the launch traced here: 54.7 us
  Pallas kernels  52.5 us (95%)
  local copies, waits for them, and re-layouts  2.22 us (4%)
    pallas_call x1, Pallas kernels, body(): pl.pallas_call(functools.partial(mixer_kernel, slots, shards, ntp), out_s...  48.4 us
    pallas_call x1, Pallas kernels, body(): pl.pallas_call(order_kernel, grid_spec=pltpu.PrefetchScalarGridSpec(num_s...  4.1 us
    reshape x1, local copies, waits for them, and re-layouts, body(): gate_w = w_gate.reshape(model, 2 * heads)  2.22 us

profile of v3, /device:TPU:17, one launch (start us, length us, event | category | flops | bytes accessed | tf_op | source)
XLA Modules:
  0.0 54.7 jit_solution(14714846705946842340)
XLA Ops:
  0.0 2.2 %copy.11.wg_hbm = bf16[4096,16]{1,0:T(8,128)(2,1)} copy(bf16[4096,16]{0,1:T(8,128)(2,1)} %bitcast.2) | data formatting | bytes 262144 | tf_op jit(solution)/shard_map/reshape | solution.py:499
  2.2 48.4 %shard_map.91.ranked_ref = bf16[4,32,4096]{2,1,0:T(8,128)(2,1)} custom-call(s32[4]{0:T(128)} %len_ref.3, s32[4,16,8]{2,1,0:T(8,128)} %bitcast.3, f32[2,32,64]{2,1,0:T(8,128)} %pool_in.1, bf16[128,4,4096]{2,1,0:T(4,128)(2,1)} %tok_hbm.1, bf16[4096,512]{1,0:T(8,128)(2,1)} %wq_hbm.1, bf16[4096,512]{1,0:T(8,128)(2,1)} %wk_hbm.1, bf16[4096,512]{1,0:T(8,128)(2,1)} %wv_hbm.1, ...), custom_call_target="tpu_custom_call" | custom-call | tf_op jit(solution)/shard_map/pallas_call | solution.py:507
  50.6 4.1 %shard_map.92 = bf16[32,4,4096]{2,1,0:T(4,128)(2,1)} custom-call(s32[4]{0:T(128)} %len_ref.3, bf16[4,32,4096]{2,1,0:T(8,128)(2,1)} %shard_map.91.ranked_ref), custom_call_target="tpu_custom_call" | custom-call | tf_op jit(solution)/shard_map/pallas_call | solution.py:550
